TPU v7x, 32 devices: a whole 2x2x4 slice. The times are simulated.
32 devices in a mesh: ep: 8 (over z, core), tp: 4 (over y, x).
Axes of the slice: x: 2, y: 2, z: 4, core: 2. Of those that a mesh axis runs over, the one named last changes fastest.
Arguments:
- tokens: bfloat16 [512, 2048], P('ep', 'tp'), as said below
- mix_gain: float32 [2048], replicated, may hold values from 0.1 to 1.9
- w_in: bfloat16 [2048, 1024], P(None, 'tp'), may hold values from -0.125 to 0.125
- a_real: float32 [64, 64], P('tp'), may hold values from -1 to -0.1
- a_imag: float32 [64, 64], P('tp'), may hold values from -3.140625 to 3.140625
- log_step: float32 [64], P('tp'), may hold values from -3 to 0
- b_coef: float32 [2, 64, 64, 16], P(None, 'tp'), may hold values from -2.5 to 2.5
- output_coefficients: float32 [2, 64, 16, 64], P(None, 'tp'), may hold values from -1.25 to 1.25
- skip: float32 [1024], P('tp'), may hold values from -6 to 6
- w_out: bfloat16 [1024, 2048], P('tp'), may hold values from -0.1875 to 0.1875
- state: float32 [2, 512, 64, 64], P(None, 'ep', 'tp'), may hold values from -6 to 6
- ffn_gain: float32 [2048], replicated, may hold values from 0.1 to 1.9
- w_gate: bfloat16 [16, 2048, 4096], P('ep', None, 'tp'), may hold values from -0.125 to 0.125
- w_up: bfloat16 [16, 2048, 4096], P('ep', None, 'tp'), may hold values from -0.125 to 0.125
- w_down: bfloat16 [16, 4096, 2048], P('ep', 'tp'), may hold values from -0.09375 to 0.09375
- expert_ids: int32 [512, 2], P('ep'), may hold values from 0 to 15, all different within a row; in each aligned block of 64 rows (0 to 63, 64 to 127, ...) at most 16 rows name the same one
- route_weights: float32 [512, 2], P('ep'), may hold values from 0.3 to 1
Outputs:
- out: bfloat16 [512, 2048], P('ep', 'tp')
- new_state: float32 [2, 512, 64, 64], P(None, 'ep', 'tp')
Inputs may be any that keep to these rules, and one draw needn't show every extreme that they name: `expert_ids`: A token's 2 experts differ. Among the 64 rows of one index of ep no expert is named more than 16 times, a bound that some block reaches. `tokens`: feature scales differ along the model width.
All inputs are finite; a program needn't handle non-finite values.
Results may differ from a plain program's by a relative error of at most 0.007.
Values may be sent and summed in bfloat16 or wider, within the bound.
A program may use at most 64 MiB of HBM per device.

v0:
```python
import jax
import jax.numpy as jnp
from jax import lax
from jax.sharding import PartitionSpec as P

epsilon = 1e-06
highest_precision = lax.Precision.HIGHEST


def rms_norm(values, gain):
    scaled = values * lax.rsqrt(jnp.mean(values * values, axis=-1, keepdims=True) + epsilon)
    return scaled * gain


def state_update(drive, a_real, a_imag, log_step, b_coef, output_coefficients, skip, state):
    count = drive.shape[0]
    groups = a_real.shape[0]
    drive_float = drive.astype(jnp.float32)
    grouped = drive_float.reshape(count, groups, -1)
    step_size = jnp.exp(log_step)[:, None]
    magnitude = jnp.exp(step_size * a_real)
    decay_re = magnitude * jnp.cos(step_size * a_imag)
    decay_imaginary = magnitude * jnp.sin(step_size * a_imag)
    denominator = a_real * a_real + a_imag * a_imag
    shifted = decay_re - 1.0
    factor_re = (shifted * a_real + decay_imaginary * a_imag) / denominator
    factor_im = (decay_imaginary * a_real - shifted * a_imag) / denominator
    coef_re = factor_re[..., None] * b_coef[0] - factor_im[..., None] * b_coef[1]
    coefficient_imaginary = factor_re[..., None] * b_coef[1] + factor_im[..., None] * b_coef[0]
    push_re = jnp.einsum("gpc,sgc->sgp", coef_re, grouped, precision=highest_precision)
    push_im = jnp.einsum(
        "gpc,sgc->sgp", coefficient_imaginary, grouped, precision=highest_precision
    )
    state_real = decay_re * state[0] - decay_imaginary * state[1] + push_re
    state_imaginary = decay_re * state[1] + decay_imaginary * state[0] + push_im
    state_readout = jnp.einsum(
        "amz,daz->dam", output_coefficients[0], state_real, precision=highest_precision
    ) - jnp.einsum(
        "amz,daz->dam", output_coefficients[1], state_imaginary, precision=highest_precision
    )
    mixed = state_readout.reshape(count, -1) + skip * drive_float
    return (jax.nn.gelu(mixed).astype(jnp.bfloat16), jnp.stack([state_real, state_imaginary]))


def slot_table(expert_ids, experts, capacity):
    flat_ids = expert_ids.reshape(-1)
    onehot = (flat_ids[:, None] == jnp.arange(experts, dtype=jnp.int32)[None, :]).astype(jnp.int32)
    ranks = jnp.cumsum(onehot, axis=0) - 1
    slot_rank = jnp.sum(onehot * ranks, axis=1)
    slots = flat_ids * capacity + slot_rank
    return (slots[:, None] == jnp.arange(experts * capacity, dtype=jnp.int32)[None, :]).astype(
        jnp.float32
    )


def local(
    tokens,
    mix_gain,
    w_in,
    a_real,
    a_imag,
    log_step,
    b_coef,
    output_coefficients,
    skip,
    w_out,
    state,
    ffn_gain,
    w_gate,
    w_up,
    w_down,
    expert_ids,
    route_weights,
):
    seq_count = tokens.shape[0]
    width = tokens.shape[1]
    top_count = expert_ids.shape[1]
    ep_count = lax.axis_size("ep")
    tp_count = lax.axis_size("tp")
    model_width = width * tp_count
    local_experts = w_gate.shape[0]
    experts = local_experts * ep_count
    capacity = max(2, 2 * seq_count * top_count // experts)
    col_start = lax.axis_index("tp") * width
    whole_rows = lax.all_gather(tokens, "tp", axis=1, tiled=True)
    tok_float = whole_rows.astype(jnp.float32)
    normed = rms_norm(tok_float, mix_gain).astype(jnp.bfloat16)
    drive = jnp.dot(normed, w_in, preferred_element_type=jnp.float32).astype(jnp.bfloat16)
    mixed, new_state = state_update(
        drive, a_real, a_imag, log_step, b_coef, output_coefficients, skip, state
    )
    partial_mix = jnp.dot(mixed, w_out, preferred_element_type=jnp.float32)
    placed = slot_table(expert_ids, experts, capacity)
    per_token = (
        placed.reshape(seq_count, top_count, experts * capacity).sum(axis=1).astype(jnp.bfloat16)
    )
    mix_full = lax.psum(partial_mix, "tp")
    resid_full = (tok_float + mix_full).astype(jnp.bfloat16)
    normed2 = rms_norm(resid_full.astype(jnp.float32), ffn_gain).astype(jnp.bfloat16)
    resid_own = lax.dynamic_slice_in_dim(resid_full, col_start, width, 1)
    send_buffer = jnp.dot(per_token.T, normed2, preferred_element_type=jnp.float32).astype(
        jnp.bfloat16
    )
    send_buffer = send_buffer.reshape(ep_count, local_experts, capacity, model_width)
    slot_rows = lax.all_to_all(send_buffer, "ep", split_axis=0, concat_axis=0, tiled=True)
    gate_vals = jnp.einsum("njcd,jdf->njcf", slot_rows, w_gate, preferred_element_type=jnp.float32)
    up_vals = jnp.einsum("njcd,jdf->njcf", slot_rows, w_up, preferred_element_type=jnp.float32)
    hidden = (jax.nn.silu(gate_vals) * up_vals).astype(jnp.bfloat16)
    partial_out = jnp.einsum("njcf,jfd->njcd", hidden, w_down, preferred_element_type=jnp.float32)
    expert_result = lax.psum_scatter(
        partial_out.astype(jnp.bfloat16), "tp", scatter_dimension=3, tiled=True
    )
    returned_rows = lax.all_to_all(expert_result, "ep", split_axis=0, concat_axis=0, tiled=True)
    returned_rows = returned_rows.reshape(experts * capacity, width).astype(jnp.float32)
    weighted = placed * route_weights.reshape(-1)[:, None]
    combined = jnp.dot(weighted, returned_rows, precision=highest_precision)
    combined = combined.reshape(seq_count, top_count, width).sum(axis=1)
    out = (resid_own.astype(jnp.float32) + combined).astype(jnp.bfloat16)
    return (out, new_state)


def solution(mesh):
    in_specs = (
        P("ep", "tp"),
        P(),
        P(None, "tp"),
        P("tp", None),
        P("tp", None),
        P("tp"),
        P(None, "tp", None, None),
        P(None, "tp", None, None),
        P("tp"),
        P("tp", None),
        P(None, "ep", "tp", None),
        P(),
        P("ep", None, "tp"),
        P("ep", None, "tp"),
        P("ep", "tp", None),
        P("ep", None),
        P("ep", None),
    )
    out_specs = (P("ep", "tp"), P(None, "ep", "tp", None))
    return jax.shard_map(local, mesh=mesh, in_specs=in_specs, out_specs=out_specs, check_vma=False)
```

profile of v0, /device:TPU:0, one launch (start us, length us, event | category | flops | bytes accessed | tf_op | source)
XLA Modules:
  0.0 168.2 jit_solution(7657873128458054456)
XLA Ops:
  7.2 0.0 copy-start
  7.2 0.0 copy-start.1
  7.2 0.0 copy-start.5
  7.2 0.0 copy-start.3
  7.2 0.0 copy-start.2
  7.2 0.0 all-reduce.2.cloned.1.call-start
  7.3 10.9 %all_gather.3 = bf16[64,2048]{1,0:T(8,128)(2,1)S(1)} all-gather(bf16[64,512]{1,0:T(8,128)(2,1)} %param.17), channel_id=1, replica_groups=mesh['ep'=8,'tp'=4] {'tp'}, dimensions={1}, use_global_device_ids=true | all-gather | bytes 327680 | tf_op jit(solution)/shard_map/all_gather | solution.py:85
  18.2 0.2 fusion.31
  18.3 1.6 convolution_convert_fusion.1
  19.9 0.1 copy.68
  20.0 0.7 exp.10
  20.7 1.3 fusion.87
  22.0 0.8 fusion.80
  22.8 1.6 fusion.24
  24.4 1.6 fusion.25
  26.1 1.8 %fusion.43 = f32[16,64,16]{1,2,0:T(8,128)S(1)} fusion(f32[64,16,64]{2,0,1:T(8,128)S(1)} %fusion.25, f32[2,16,16,64]{3,2,1,0:T(8,128)} %param.24), kind=kOutput, calls=%fused_computation.43 | convolution fusion | flops 12582912 | bytes 458752 | tf_op jit(solution)/shard_map/amz,daz->dam/dot_general | solution.py:36
  27.9 0.9 convolution_subtract_fusion
  28.9 0.1 copy.69
  29.0 1.1 fusion.72
  30.1 0.0 all-reduce.2.cloned.1.call-update
  30.1 0.0 reduce-scatter.2.cloned.1.call-start
  30.1 0.1 copy.70
  30.2 0.1 eq.49
  30.4 0.1 fusion.67
  30.5 0.2 reduce_window_sum.11
  30.6 0.2 select_reduce_fusion
  30.8 0.1 reduce_sum.49
  31.0 0.1 copy.71
  31.0 0.1 convert_reduce_fusion
  31.2 44.7 %all-reduce.2.cloned.1.call-done = f32[64,2048]{1,0:T(8,128)} async-done(((f32[64,2048]{1,0:T(8,128)}), f32[64,2048]{1,0:T(8,128)}) %all-reduce.2.cloned.1.call-update) | async-done | bytes 524304 | tf_op jit(solution)/shard_map/psum | solution.py:97
  75.9 1.2 fusion.28
  77.1 0.5 convolution_convert_fusion
  77.6 0.0 slice-start.2
  77.6 31.2 %all_to_all.10 = bf16[8,2,16,2048]{3,2,1,0:T(8,128)(2,1)S(1)} all-to-all(bf16[8,2,16,2048]{3,2,1,0:T(8,128)(2,1)S(1)} %bitcast.107), channel_id=1, replica_groups=mesh['ep'=8,'tp'=4] {'ep'}, dimensions={0} | all-to-all | bytes 2097152 | tf_op jit(solution)/shard_map/all_to_all | solution.py:105
  108.9 4.8 %fusion.12 = f32[8,2,16,1024]{3,2,0,1:T(8,128)S(1)} fusion(bf16[2,2048,1024]{2,1,0:T(8,128)(2,1)} %param.29, bf16[8,2,16,2048]{3,2,1,0:T(8,128)(2,1)S(1)} %all_to_all.10), kind=kOutput, calls=%fused_computation.9 | convolution fusion | flops 1073741824 | bytes 10485760 | tf_op jit(solution)/shard_map/njcd,jdf->njcf/dot_general | solution.py:106
  113.7 0.0 slice-start.1
  113.7 1.4 fusion.21
  115.1 1.0 slice-done.1
  116.1 2.2 %fusion.9 = bf16[8,2,16,2048]{3,2,0,1:T(8,128)(2,1)} fusion(bf16[8,2,16,1024]{3,2,0,1:T(8,128)(2,1)S(1)} %fusion.21, bf16[2,1024,2048]{2,1,0:T(8,128)(2,1)S(1)} %bitcast.104), kind=kOutput, calls=%fused_computation.8 | convolution fusion | flops 1074266112 | bytes 9961472 | tf_op jit(solution)/shard_map/njcf,jfd->njcd/dot_general | solution.py:109
  118.4 0.0 reduce-scatter.2.cloned.1.call-update
  118.4 26.0 %reduce-scatter.2.cloned.1.call-done = bf16[8,2,16,512]{3,2,0,1:T(8,128)(2,1)} async-done(((bf16[8,2,16,2048]{3,2,0,1:T(8,128)(2,1)}), bf16[8,2,16,512]{3,2,0,1:T(8,128)(2,1)}) %reduce-scatter.2.cloned.1.call-update) | async-done | bytes 262160 | tf_op jit(solution)/shard_map/reduce_scatter | solution.py:110
  144.4 1.7 copy.74
  146.1 4.6 %all-to-all-start.1 = ((bf16[8,2,16,512]{3,2,1,0:T(8,128)(2,1)}), bf16[8,2,16,512]{3,2,1,0:T(8,128)(2,1)S(1)}, u32[]{:S(2)}, u32[]{:S(2)}) async-start(bf16[8,2,16,512]{3,2,1,0:T(8,128)(2,1)} %copy.74), calls=%async_computation.2 | async-start | bytes 524288 | tf_op jit(solution)/shard_map/all_to_all | solution.py:113
  150.7 0.1 pad_maximum_fusion
  150.8 1.6 copy.75
  152.4 8.0 %all-to-all-done.1 = bf16[8,2,16,512]{3,2,1,0:T(8,128)(2,1)S(1)} async-done(((bf16[8,2,16,512]{3,2,1,0:T(8,128)(2,1)}), bf16[8,2,16,512]{3,2,1,0:T(8,128)(2,1)S(1)}, u32[]{:S(2)}, u32[]{:S(2)}) %all-to-all-start.1) | async-done | bytes 262176 | tf_op jit(solution)/shard_map/all_to_all | solution.py:113
  160.4 0.3 convolution_reduce_fusion
  160.8 0.7 add_convert_fusion
  (17 shorter events, 0.0 us)
Async XLA Ops:
  7.2 21.8 %copy-start = (bf16[256,2048]{1,0:T(8,128)(2,1)S(1)}, bf16[256,2048]{1,0:T(8,128)(2,1)}, u32[]{:S(2)}) copy-start(bf16[256,2048]{1,0:T(8,128)(2,1)} %param.26) | copy-start | bytes 3145732
  7.2 20.7 %copy-start.1 = (f32[2,16,16,64]{3,2,1,0:T(8,128)S(1)}, f32[2,16,16,64]{3,2,1,0:T(8,128)}, u32[]{:S(2)}) copy-start(f32[2,16,16,64]{3,2,1,0:T(8,128)} %param.24) | copy-start | bytes 393220
  7.2 21.8 %copy-start.5 = (f32[256]{0:T(256)S(1)}, f32[256]{0:T(256)}, u32[]{:S(2)}) copy-start(f32[256]{0:T(256)} %param.25) | copy-start | bytes 3076
  7.2 22.9 %copy-start.3 = (s32[64,2]{0,1:T(2,128)S(1)}, s32[64,2]{0,1:T(2,128)}, u32[]{:S(2)}) copy-start(s32[64,2]{0,1:T(2,128)} %param.32) | copy-start | bytes 1540
  7.2 69.9 %copy-start.2 = (f32[2048]{0:T(1024)S(1)}, f32[2048]{0:T(1024)}, u32[]{:S(2)}) copy-start(f32[2048]{0:T(1024)} %param.28) | copy-start | bytes 24580
  7.2 68.7 %all-reduce.2.cloned.1.call-start = ((), (), s32[]{:S(2)}) async-start(), calls=%async_computation.3 | async-start | bytes 1048576 | tf_op jit(solution)/shard_map/psum | solution.py:97
  30.1 114.4 %reduce-scatter.2.cloned.1.call-start = ((), (), s32[]{:S(2)}) async-start(), calls=%async_computation.4 | async-start | bytes 1310720 | tf_op jit(solution)/shard_map/reduce_scatter | solution.py:110
  77.6 36.0 %slice-start.2 = ((s8[8388608]{0:T(1024)(128)(4,1)}), s8[4194304]{0:T(1024)(128)(4,1)S(1)}, s32[]{:S(2)}) async-start(s8[8388608]{0:T(1024)(128)(4,1)} %bitcast.112), calls=%async_computation.7 | async-start | bytes 8388608
  108.9 4.8 %slice-start.3 = ((s8[8388608]{0:T(1024)(128)(4,1)}), s8[4194304]{0:T(1024)(128)(4,1)S(1)}, s32[]{:S(2)}) async-start(s8[8388608]{0:T(1024)(128)(4,1)} %bitcast.112), calls=%async_computation.8 | async-start | bytes 8388608
  108.9 6.3 %slice-start = ((s8[8388608]{0:T(1024)(128)(4,1)}), s8[4194304]{0:T(1024)(128)(4,1)S(1)}, s32[]{:S(2)}) async-start(s8[8388608]{0:T(1024)(128)(4,1)} %bitcast.103), calls=%async_computation.5 | async-start | bytes 8388608
  113.7 2.5 %slice-start.1 = ((s8[8388608]{0:T(1024)(128)(4,1)}), s8[4194304]{0:T(1024)(128)(4,1)S(1)}, s32[]{:S(2)}) async-start(s8[8388608]{0:T(1024)(128)(4,1)} %bitcast.103), calls=%async_computation.6 | async-start | bytes 8388608
  116.1 44.3 %copy-start.4 = (f32[64,2]{0,1:T(2,128)S(1)}, f32[64,2]{0,1:T(2,128)}, u32[]{:S(2)}) copy-start(f32[64,2]{0,1:T(2,128)} %param.33) | copy-start | bytes 1540
  146.1 14.3 %all-to-all-start.1 = ((bf16[8,2,16,512]{3,2,1,0:T(8,128)(2,1)}), bf16[8,2,16,512]{3,2,1,0:T(8,128)(2,1)S(1)}, u32[]{:S(2)}, u32[]{:S(2)}) async-start(bf16[8,2,16,512]{3,2,1,0:T(8,128)(2,1)} %copy.74), calls=%async_computation.2 | async-start | bytes 524288 | tf_op jit(solution)/shard_map/all_to_all | solution.py:113
Sparse Core Ops, SparseCore 0:
  30.2 45.6 all-reduce.1
  118.5 25.8 reduce-scatter.1
where the time goes:
time: 169 us; the launch traced here: 168 us
  waiting for transfers between devices  78.8 us (47%)
  blocking collectives  42.1 us (25%)
  matrix products  18 us (11%)
  between operations  14.3 us (8%)
  local copies, waits for them, and re-layouts  6.87 us (4%)
  starting transfers between devices  4.69 us (3%)
  other arithmetic  3.53 us (2%)
    psum x1, waiting for transfers between devices, local(): mix_full = lax.psum(partial_mix, 'tp')  44.7 us
    all_to_all x1, blocking collectives, local(): lax.all_to_all(send_buffer, 'ep', split_axis=0, concat_axis=0, tiled=True)  31.2 us
    reduce_scatter x1, waiting for transfers between devices, local(): lax.psum_scatter(partial_out.astype(jnp.bfloat16), 'tp', scatter_dimensio...  26 us
    all_gather x1, blocking collectives, local(): whole_rows = lax.all_gather(tokens, 'tp', axis=1, tiled=True)  10.9 us
    all_to_all x1, waiting for transfers between devices, local(): lax.all_to_all(expert_result, 'ep', split_axis=0, concat_axis=0, tiled=True)  8.01 us
    dot_general x1, matrix products, local(): jnp.einsum('njcd,jdf->njcf', slot_rows, w_gate, preferred_element_type=jn...  4.78 us
    all_to_all x1, starting transfers between devices, local(): lax.all_to_all(expert_result, 'ep', split_axis=0, concat_axis=0, tiled=True)  4.61 us
  transfers between devices with their start and end apart: 3, of which 3 were waited for; matrix products, arithmetic and copies ran while one was open for 2% of the time, Pallas kernels for 0%

commit v1 on v0

--- a/solution.py
+++ b/solution.py
@@ -82,7 +82,12 @@
     experts = local_experts * ep_count
     capacity = max(2, 2 * seq_count * top_count // experts)
     col_start = lax.axis_index("tp") * width
-    whole_rows = lax.all_gather(tokens, "tp", axis=1, tiled=True)
+    ring = [tokens]
+    for hop in range(3):
+        ring.append(lax.ppermute(ring[-1], "tp", [(dev, (dev + 1) % 4) for dev in range(4)]))
+    whole_rows = jnp.roll(
+        jnp.concatenate(ring[::-1], axis=1), (lax.axis_index("tp") + 1) * ring[0].shape[1], axis=1
+    )
     tok_float = whole_rows.astype(jnp.float32)
     normed = rms_norm(tok_float, mix_gain).astype(jnp.bfloat16)
     drive = jnp.dot(normed, w_in, preferred_element_type=jnp.float32).astype(jnp.bfloat16)

time: 169 us -> 175 us (1.036)
  blocking collectives: 42.1 us -> 31.2 us
  waiting for transfers between devices: 78.8 us -> 88.3 us
  starting transfers between devices: 4.69 us -> 9 us
  local copies, waits for them, and re-layouts: 6.87 us -> 9.9 us
    all_gather x1 -> x0, blocking collectives: 10.9 us -> none  [local(): whole_rows = lax.all_gather(tokens, 'tp', axis=1, tiled=True)]
    ppermute x0 -> x3, waiting for transfers between devices: none -> 8.75 us  [local(): lax.ppermute(ring[-1], 'tp', [(dev, (dev + 1) % 4) for dev in range(4)])]
    ppermute x0 -> x3, starting transfers between devices: none -> 4.31 us  [local(): lax.ppermute(ring[-1], 'tp', [(dev, (dev + 1) % 4) for dev in range(4)])]
    unnamed x22 -> x29, local copies, waits for them, and re-layouts: 2.74 us -> 4.92 us
  transfers between devices with their start and end apart: 3 -> 6, of which waited for: 3 -> 6; matrix products, arithmetic and copies ran while one was open for 2% -> 3% of each run, Pallas kernels for 0% -> 0%
where the time goes in v1:
time: 175 us; the launch traced here: 174 us
  waiting for transfers between devices  88.3 us (50%)
  blocking collectives  31.2 us (18%)
  matrix products  17.7 us (10%)
  between operations  14.3 us (8%)
  local copies, waits for them, and re-layouts  9.9 us (6%)
  starting transfers between devices  9 us (5%)
  other arithmetic  3.55 us (2%)
    psum x1, waiting for transfers between devices, local(): mix_full = lax.psum(partial_mix, 'tp')  45.5 us
    all_to_all x1, blocking collectives, local(): lax.all_to_all(send_buffer, 'ep', split_axis=0, concat_axis=0, tiled=True)  31.2 us
    reduce_scatter x1, waiting for transfers between devices, local(): lax.psum_scatter(partial_out.astype(jnp.bfloat16), 'tp', scatter_dimensio...  26 us
    ppermute x3, waiting for transfers between devices, local(): lax.ppermute(ring[-1], 'tp', [(dev, (dev + 1) % 4) for dev in range(4)])  8.75 us
    all_to_all x1, waiting for transfers between devices, local(): lax.all_to_all(expert_result, 'ep', split_axis=0, concat_axis=0, tiled=True)  8.05 us
    unnamed x29, local copies, waits for them, and re-layouts  4.92 us
    dot_general x1, matrix products, local(): jnp.einsum('njcd,jdf->njcf', slot_rows, w_gate, preferred_element_type=jn...  4.78 us
    all_to_all x1, starting transfers between devices, local(): lax.all_to_all(expert_result, 'ep', split_axis=0, concat_axis=0, tiled=True)  4.61 us
  transfers between devices with their start and end apart: 6, of which 6 were waited for; matrix products, arithmetic and copies ran while one was open for 3% of the time, Pallas kernels for 0%

profile of v1, /device:TPU:0, one launch (start us, length us, event | category | flops | bytes accessed | tf_op | source)
XLA Modules:
  0.0 174.1 jit_solution(16253391379168906446)
XLA Ops:
  7.2 0.0 all-reduce.2.cloned.1.call-start
  7.3 3.0 %collective-permute-start = (bf16[64,512]{1,0:T(8,128)(2,1)}, bf16[64,512]{1,0:T(8,128)(2,1)S(1)}, u32[]{:S(2)}, u32[]{:S(2)}) collective-permute-start(bf16[64,512]{1,0:T(8,128)(2,1)} %param.17), channel_id=1, source_target_pairs={{0,1},{1,2},{2,3},{3,0},{4,5},{5,6},{6,7},{7,4},{8,9},{9,10},{10,1... | collective-permute-start | bytes 196616 | tf_op jit(solution)/shard_map/ppermute | solution.py:87
  10.3 3.4 %collective-permute-done = bf16[64,512]{1,0:T(8,128)(2,1)S(1)} collective-permute-done((bf16[64,512]{1,0:T(8,128)(2,1)}, bf16[64,512]{1,0:T(8,128)(2,1)S(1)}, u32[]{:S(2)}, u32[]{:S(2)}) %collective-permute-start) | collective-permute-done | bytes 65568 | tf_op jit(solution)/shard_map/ppermute | solution.py:87
  13.7 1.1 collective-permute-start.1
  14.8 1.3 fusion.89
  16.0 0.7 exp.10
  16.7 2.2 %collective-permute-done.1 = bf16[64,512]{1,0:T(8,128)(2,1)S(1)} collective-permute-done((bf16[64,512]{1,0:T(8,128)(2,1)S(1)}, bf16[64,512]{1,0:T(8,128)(2,1)S(1)}, u32[]{:S(2)}, u32[]{:S(2)}) %collective-permute-start.1) | collective-permute-done | bytes 65568 | tf_op jit(solution)/shard_map/ppermute | solution.py:87
  18.9 0.2 collective-permute-start.2
  19.1 0.8 fusion.81
  19.9 0.8 copy.70
  20.7 0.1 eq.52
  20.9 3.2 %collective-permute-done.2 = bf16[64,512]{1,0:T(8,128)(2,1)S(1)} collective-permute-done((bf16[64,512]{1,0:T(8,128)(2,1)S(1)}, bf16[64,512]{1,0:T(8,128)(2,1)S(1)}, u32[]{:S(2)}, u32[]{:S(2)}) %collective-permute-start.2) | collective-permute-done | bytes 65568 | tf_op jit(solution)/shard_map/ppermute | solution.py:87
  24.1 0.8 constant_dynamic-update-slice_fusion.4
  24.9 0.8 constant_dynamic-update-slice_fusion
  25.8 0.2 fusion.31
  25.9 0.6 copy-done.1
  26.6 1.6 convolution_convert_fusion.1
  28.2 0.1 copy.68
  28.3 1.6 fusion.24
  29.9 1.6 fusion.25
  31.6 0.9 fusion.44
  32.5 0.9 convolution_subtract_fusion
  33.4 0.1 copy.69
  33.5 1.8 %fusion.73 = f32[64,2048]{1,0:T(8,128)} fusion(bf16[256,2048]{1,0:T(8,128)(2,1)S(1)} %copy-done, f32[64,256]{1,0:T(8,128)S(1)} %copy.69, bf16[64,256]{1,0:T(8,128)(2,1)S(1)} %convolution_convert_fusion.1, f32[256]{0:T(256)} %param.25), kind=kOutput, calls=%fused_computation.82 | convolution fusion | flops 67305472 | bytes 1672192 | tf_op jit(solution)/shard_map/dot_general | solution.py:97
  35.3 0.0 reduce-scatter.2.cloned.1.call-start
  35.4 0.1 fusion.68
  35.5 0.2 reduce_window_sum.11
  35.6 0.2 select_reduce_fusion
  35.8 0.1 reduce_sum.49
  36.0 0.1 copy.71
  36.0 0.1 convert_reduce_fusion
  36.1 45.5 %all-reduce.2.cloned.1.call-done = f32[64,2048]{1,0:T(8,128)} async-done(((f32[64,2048]{1,0:T(8,128)}), f32[64,2048]{1,0:T(8,128)}) %all-reduce.2.cloned.1.call-update) | async-done | bytes 524304 | tf_op jit(solution)/shard_map/psum | solution.py:102
  81.6 1.3 fusion.28
  82.9 0.5 convolution_convert_fusion
  83.4 31.2 %all_to_all.10 = bf16[8,2,16,2048]{3,2,1,0:T(8,128)(2,1)S(1)} all-to-all(bf16[8,2,16,2048]{3,2,1,0:T(8,128)(2,1)S(1)} %bitcast.107), channel_id=1, replica_groups=mesh['ep'=8,'tp'=4] {'ep'}, dimensions={0} | all-to-all | bytes 2097152 | tf_op jit(solution)/shard_map/all_to_all | solution.py:110
  114.7 4.8 %fusion.12 = f32[8,2,16,1024]{3,2,0,1:T(8,128)S(1)} fusion(bf16[2,2048,1024]{2,1,0:T(8,128)(2,1)} %param.29, bf16[8,2,16,2048]{3,2,1,0:T(8,128)(2,1)S(1)} %all_to_all.10), kind=kOutput, calls=%fused_computation.9 | convolution fusion | flops 1073741824 | bytes 10485760 | tf_op jit(solution)/shard_map/njcd,jdf->njcf/dot_general | solution.py:111
  119.5 1.4 fusion.21
  121.0 1.0 slice-done.1
  122.0 2.2 %fusion.9 = bf16[8,2,16,2048]{3,2,0,1:T(8,128)(2,1)} fusion(bf16[8,2,16,1024]{3,2,0,1:T(8,128)(2,1)S(1)} %fusion.21, bf16[2,1024,2048]{2,1,0:T(8,128)(2,1)S(1)} %bitcast.104), kind=kOutput, calls=%fused_computation.8 | convolution fusion | flops 1074266112 | bytes 9961472 | tf_op jit(solution)/shard_map/njcf,jfd->njcd/dot_general | solution.py:114
  124.2 0.0 reduce-scatter.2.cloned.1.call-update
  124.2 26.0 %reduce-scatter.2.cloned.1.call-done = bf16[8,2,16,512]{3,2,0,1:T(8,128)(2,1)} async-done(((bf16[8,2,16,2048]{3,2,0,1:T(8,128)(2,1)}), bf16[8,2,16,512]{3,2,0,1:T(8,128)(2,1)}) %reduce-scatter.2.cloned.1.call-update) | async-done | bytes 262160 | tf_op jit(solution)/shard_map/reduce_scatter | solution.py:115
  150.3 1.7 copy.74
  151.9 4.6 %all-to-all-start.1 = ((bf16[8,2,16,512]{3,2,1,0:T(8,128)(2,1)}), bf16[8,2,16,512]{3,2,1,0:T(8,128)(2,1)S(1)}, u32[]{:S(2)}, u32[]{:S(2)}) async-start(bf16[8,2,16,512]{3,2,1,0:T(8,128)(2,1)} %copy.74), calls=%async_computation.2 | async-start | bytes 524288 | tf_op jit(solution)/shard_map/all_to_all | solution.py:118
  156.5 0.1 pad_maximum_fusion
  156.6 1.6 copy.75
  158.2 8.0 %all-to-all-done.1 = bf16[8,2,16,512]{3,2,1,0:T(8,128)(2,1)S(1)} async-done(((bf16[8,2,16,512]{3,2,1,0:T(8,128)(2,1)}), bf16[8,2,16,512]{3,2,1,0:T(8,128)(2,1)S(1)}, u32[]{:S(2)}, u32[]{:S(2)}) %all-to-all-start.1) | async-done | bytes 262176 | tf_op jit(solution)/shard_map/all_to_all | solution.py:118
  166.3 0.3 convolution_reduce_fusion
  166.6 0.7 add_convert_fusion
  (30 shorter events, 0.1 us)
Async XLA Ops:
  7.2 26.4 %copy-start = (bf16[256,2048]{1,0:T(8,128)(2,1)S(1)}, bf16[256,2048]{1,0:T(8,128)(2,1)}, u32[]{:S(2)}) copy-start(bf16[256,2048]{1,0:T(8,128)(2,1)} %param.26) | copy-start | bytes 3145732
  7.2 28.9 %copy-start.4 = (s32[64,2]{0,1:T(2,128)S(1)}, s32[64,2]{0,1:T(2,128)}, u32[]{:S(2)}) copy-start(s32[64,2]{0,1:T(2,128)} %param.32) | copy-start | bytes 1540
  7.2 24.4 %copy-start.2 = (f32[2,16,16,64]{3,2,1,0:T(8,128)S(1)}, f32[2,16,16,64]{3,2,1,0:T(8,128)}, u32[]{:S(2)}) copy-start(f32[2,16,16,64]{3,2,1,0:T(8,128)} %param.24) | copy-start | bytes 393220
  7.2 75.7 %copy-start.3 = (f32[2048]{0:T(1024)S(1)}, f32[2048]{0:T(1024)}, u32[]{:S(2)}) copy-start(f32[2048]{0:T(1024)} %param.28) | copy-start | bytes 24580
  7.2 74.4 %all-reduce.2.cloned.1.call-start = ((), (), s32[]{:S(2)}) async-start(), calls=%async_computation.3 | async-start | bytes 1048576 | tf_op jit(solution)/shard_map/psum | solution.py:102
  7.3 6.4 %collective-permute-start = (bf16[64,512]{1,0:T(8,128)(2,1)}, bf16[64,512]{1,0:T(8,128)(2,1)S(1)}, u32[]{:S(2)}, u32[]{:S(2)}) collective-permute-start(bf16[64,512]{1,0:T(8,128)(2,1)} %param.17), channel_id=1, source_target_pairs={{0,1},{1,2},{2,3},{3,0},{4,5},{5,6},{6,7},{7,4},{8,9},{9,10},{10,1... | collective-permute-start | bytes 196616 | tf_op jit(solution)/shard_map/ppermute | solution.py:87
  13.7 5.2 %collective-permute-start.1 = (bf16[64,512]{1,0:T(8,128)(2,1)S(1)}, bf16[64,512]{1,0:T(8,128)(2,1)S(1)}, u32[]{:S(2)}, u32[]{:S(2)}) collective-permute-start(bf16[64,512]{1,0:T(8,128)(2,1)S(1)} %collective-permute-done), channel_id=1, source_target_pairs={{0,1},{1,2},{2,3},{3,0},{4,5},{5,6},{6,7},{7,4},{8,9},{9,10},{10,1... | collective-permute-start | bytes 196616 | tf_op jit(solution)/shard_map/ppermute | solution.py:87
  18.9 5.2 %collective-permute-start.2 = (bf16[64,512]{1,0:T(8,128)(2,1)S(1)}, bf16[64,512]{1,0:T(8,128)(2,1)S(1)}, u32[]{:S(2)}, u32[]{:S(2)}) collective-permute-start(bf16[64,512]{1,0:T(8,128)(2,1)S(1)} %collective-permute-done.1), channel_id=1, source_target_pairs={{0,1},{1,2},{2,3},{3,0},{4,5},{5,6},{6,7},{7,4},{8,9},{9,10},{10,1... | collective-permute-start | bytes 196616 | tf_op jit(solution)/shard_map/ppermute | solution.py:87
  25.8 0.8 copy-start.1
  35.3 114.9 %reduce-scatter.2.cloned.1.call-start = ((), (), s32[]{:S(2)}) async-start(), calls=%async_computation.4 | async-start | bytes 1310720 | tf_op jit(solution)/shard_map/reduce_scatter | solution.py:115
  83.4 36.0 %slice-start.2 = ((s8[8388608]{0:T(1024)(128)(4,1)}), s8[4194304]{0:T(1024)(128)(4,1)S(1)}, s32[]{:S(2)}) async-start(s8[8388608]{0:T(1024)(128)(4,1)} %bitcast.112), calls=%async_computation.7 | async-start | bytes 8388608
  114.7 4.8 %slice-start.3 = ((s8[8388608]{0:T(1024)(128)(4,1)}), s8[4194304]{0:T(1024)(128)(4,1)S(1)}, s32[]{:S(2)}) async-start(s8[8388608]{0:T(1024)(128)(4,1)} %bitcast.112), calls=%async_computation.8 | async-start | bytes 8388608
  114.7 6.3 %slice-start = ((s8[8388608]{0:T(1024)(128)(4,1)}), s8[4194304]{0:T(1024)(128)(4,1)S(1)}, s32[]{:S(2)}) async-start(s8[8388608]{0:T(1024)(128)(4,1)} %bitcast.103), calls=%async_computation.5 | async-start | bytes 8388608
  119.5 2.5 %slice-start.1 = ((s8[8388608]{0:T(1024)(128)(4,1)}), s8[4194304]{0:T(1024)(128)(4,1)S(1)}, s32[]{:S(2)}) async-start(s8[8388608]{0:T(1024)(128)(4,1)} %bitcast.103), calls=%async_computation.6 | async-start | bytes 8388608
  122.0 44.3 %copy-start.5 = (f32[64,2]{0,1:T(2,128)S(1)}, f32[64,2]{0,1:T(2,128)}, u32[]{:S(2)}) copy-start(f32[64,2]{0,1:T(2,128)} %param.33) | copy-start | bytes 1540
  151.9 14.3 %all-to-all-start.1 = ((bf16[8,2,16,512]{3,2,1,0:T(8,128)(2,1)}), bf16[8,2,16,512]{3,2,1,0:T(8,128)(2,1)S(1)}, u32[]{:S(2)}, u32[]{:S(2)}) async-start(bf16[8,2,16,512]{3,2,1,0:T(8,128)(2,1)} %copy.74), calls=%async_computation.2 | async-start | bytes 524288 | tf_op jit(solution)/shard_map/all_to_all | solution.py:118
Sparse Core Ops, SparseCore 0:
  35.4 46.1 all-reduce.1
  124.3 25.8 reduce-scatter.1
